TPU v7x, 512 devices: a whole 4x4x16 slice. The times are simulated.
512 devices in a mesh: ra: 16 (over y, x), cb: 32 (over z, core).
Axes of the slice: x: 4, y: 4, z: 16, core: 2. Of those that a mesh axis runs over, the one named last changes fastest.
Arguments:
- tokens: bfloat16 [8192, 2048], P('cb', 'ra'), may hold values from -40 to 40
- gain_first: float32 [2048], replicated, may hold values from 0.1 to 1.9
- gate_first: float32 [2048, 5632], P('cb', 'ra'), may hold values from -0.125 to 0.125
- gate_first_scale: float32 [5632], P('ra'), may hold values from 0.5 to 2
- up_first: float32 [2048, 5632], P('cb', 'ra'), may hold values from -0.125 to 0.125
- up_first_scale: float32 [5632], P('ra'), may hold values from 0.5 to 2
- down_first: float32 [5632, 2048], P('ra', 'cb'), may hold values from -0.078125 to 0.078125
- down_first_scale: float32 [2048], replicated, may hold values from 0.5 to 2
- gain_second: float32 [2048], replicated, may hold values from 0.1 to 1.9
- gate_second: float32 [2048, 5632], P('cb', 'ra'), may hold values from -0.125 to 0.125
- gate_second_scale: float32 [5632], P('ra'), may hold values from 0.5 to 2
- up_second: float32 [2048, 5632], P('cb', 'ra'), may hold values from -0.125 to 0.125
- up_second_scale: float32 [5632], P('ra'), may hold values from 0.5 to 2
- down_second: float32 [5632, 2048], P('ra', 'cb'), may hold values from -0.078125 to 0.078125
- down_second_scale: float32 [2048], replicated, may hold values from 0.5 to 2
- gain_last: float32 [2048], replicated, may hold values from 0.1 to 1.9
Outputs:
- mixed: bfloat16 [8192, 2048], P('cb', 'ra')
All inputs are finite; a program needn't handle non-finite values.
Results may differ from a plain program's by a relative error of at most 0.025.
Values may be sent and summed in bfloat16 or wider, within the bound.
No kernel may reach another device: no remote copies, remote signals or barrier semaphores. Data moves between devices by JAX's collectives and lax.ppermute only.
A program may use at most 64 MiB of HBM per device.

v0:
```python
import functools

import jax
import jax.numpy as jnp
from jax import lax
from jax.sharding import Mesh
from jax.sharding import PartitionSpec as P

D = 2048
RA = ("ra_0", "ra_1")
CB = ("cb_0", "cb_1")


def in_one_piece(arrays, axis, dim, along):
    widths = [a.shape[along] for a in arrays]
    both = jnp.concatenate(arrays, axis=along)
    out = lax.all_gather(both, axis, axis=dim, tiled=True)
    return tuple(jnp.split(out, [sum(widths[:k]) for k in range(1, len(widths))], axis=along))


def in_order(pieces, dim):
    pieces = jnp.moveaxis(pieces, 0, dim)
    lengths = pieces.shape
    return pieces.reshape(*lengths[:dim], lengths[dim] * lengths[dim + 1], *lengths[dim + 2 :])


def all_blocks(x, axes, order):
    pieces = x
    for k in order:
        pieces = lax.all_gather(pieces, axes[k])
    done = order[::-1]
    back = [done.index(k) for k in range(len(axes))]
    pieces = pieces.transpose(*back, *range(len(axes), pieces.ndim))
    return pieces.reshape(-1, *x.shape)


def gather_axes(x, axes, order, dim):
    return in_order(all_blocks(x, axes, order), dim)


def in_blocks(x, dim, count):
    before, after = (x.shape[:dim], x.shape[dim + 1 :])
    return jnp.moveaxis(x.reshape(*before, count, -1, *after), dim, 0)


def sent_and_summed(x, axis, dim):
    pieces = in_blocks(x, dim, lax.axis_size(axis))
    arrived = lax.all_to_all(pieces, axis, split_axis=0, concat_axis=0, tiled=True)
    return arrived.astype(jnp.float32).sum(axis=0)


def copy_for_each(x, axis):
    copies = jnp.broadcast_to(x, (lax.axis_size(axis), *x.shape))
    return lax.all_to_all(copies, axis, split_axis=0, concat_axis=0, tiled=True)


def collect(x, axis, dim):
    pieces = copy_for_each(x, axis)
    return in_order(pieces, dim)


def by_axis(x, axes):
    return functools.reduce(lax.psum, axes, x)


def own_slice(vector, width):
    return lax.dynamic_slice_in_dim(vector, lax.axis_index(RA) * width, width, 0)


def full_norm(values, gain):
    meansq = jnp.mean(values * values, axis=1, keepdims=True)
    return (values * lax.rsqrt(meansq + 1e-06) * gain).astype(jnp.bfloat16)


def expand(normed, w_gate, s_gate, w_up, s_up, w_down):
    pieces = in_one_piece((w_gate.astype(jnp.bfloat16), w_up.astype(jnp.bfloat16)), CB, 0, 1)
    gate = jnp.dot(normed, pieces[0], preferred_element_type=jnp.float32)
    upper = jnp.dot(normed, pieces[1], preferred_element_type=jnp.float32)
    hidden = (jax.nn.silu(gate * s_gate) * (upper * s_up)).astype(jnp.bfloat16)
    return jnp.dot(
        hidden,
        gather_axes(w_down.astype(jnp.bfloat16), CB, (0, 1), 1),
        preferred_element_type=jnp.float32,
    )


def reduce_share(partial_value):
    return sent_and_summed(partial_value.astype(jnp.bfloat16), RA, 1)


def shards(
    tokens,
    gain_first,
    gate_first,
    gate_first_scale,
    up_first,
    up_first_scale,
    down_first,
    down_first_scale,
    gain_second,
    gate_second,
    gate_second_scale,
    up_second,
    up_second_scale,
    down_second,
    down_second_scale,
    gain_last,
):
    width = tokens.shape[1]
    whole_in = collect(tokens, RA, 1).astype(jnp.float32)
    normed = full_norm(whole_in, gain_first)
    partial_value = expand(
        normed, gate_first, gate_first_scale, up_first, up_first_scale, down_first
    )
    share = reduce_share(partial_value)
    first_share = 0.1 * tokens.astype(jnp.float32) + 0.5 * share * own_slice(
        down_first_scale, width
    )
    squares = by_axis(jnp.sum(first_share * first_share, axis=1), RA)
    scaled = first_share * lax.rsqrt(squares / D + 1e-06)[:, None] * own_slice(gain_second, width)
    normed_next = collect(scaled.astype(jnp.bfloat16), RA, 1)
    partial_next = expand(
        normed_next, gate_second, gate_second_scale, up_second, up_second_scale, down_second
    )
    second = 0.1 * first_share + 0.5 * reduce_share(partial_next) * own_slice(
        down_second_scale, width
    )
    closing = by_axis(jnp.sum(second * second, axis=1), RA)
    return (second * lax.rsqrt(closing / D + 1e-06)[:, None] * own_slice(gain_last, width)).astype(
        jnp.bfloat16
    )


def solution(mesh):
    torus = Mesh(mesh.devices.reshape(4, 4, 16, 2), ("ra_0", "ra_1", "cb_0", "cb_1"))
    return jax.shard_map(
        shards,
        mesh=torus,
        in_specs=(
            P(CB, RA),
            P(),
            P(CB, RA),
            P(RA),
            P(CB, RA),
            P(RA),
            P(RA, CB),
            P(),
            P(),
            P(CB, RA),
            P(RA),
            P(CB, RA),
            P(RA),
            P(RA, CB),
            P(),
            P(),
        ),
        out_specs=P(CB, RA),
        check_vma=False,
    )
```

profile of v0, /device:TPU:32, one launch (start us, length us, event | category | flops | bytes accessed | tf_op | source)
XLA Modules:
  0.0 297.0 jit_solution(3545539156918879471)
XLA Ops:
  6.5 0.9 convert_bitcast_fusion.1
  7.5 40.9 %all-gather.4 = bf16[16,352,64]{1,2,0:T(8,128)(2,1)} all-gather(bf16[1,352,64]{1,2,0:T(8,128)(2,1)S(1)} %convert_bitcast_fusion.1), channel_id=2, replica_groups=mesh['ra_0'=4,'ra_1'=4,'cb_0'=16,'cb_1'=2] {'cb_0'}, dimensions={0}, use_global_device_ids=true | all-gather | bytes 765952 | tf_op jit(solution)/shard_map/all_gather | solution.py:30
  48.5 0.0 all-gather.11.cloned.1.call-start
  48.5 0.9 convert_element_type.67
  49.4 0.9 convert_element_type.68
  50.3 0.7 pad_maximum_fusion
  51.1 0.0 all-gather.17.cloned.1.call-start
  51.1 34.0 %all-gather.5 = bf16[16,352,64]{1,2,0:T(8,128)(2,1)} all-gather(bf16[1,352,64]{1,2,0:T(8,128)(2,1)S(1)} %convert_bitcast_fusion), channel_id=4, replica_groups=mesh['ra_0'=4,'ra_1'=4,'cb_0'=16,'cb_1'=2] {'cb_0'}, dimensions={0}, use_global_device_ids=true | all-gather | bytes 765952 | tf_op jit(solution)/shard_map/all_gather | solution.py:30
  85.2 0.0 all-gather.13.cloned.1.call-start
  85.3 0.7 pad_maximum_fusion.1
  86.1 0.1 copy.23
  86.2 0.1 broadcast_in_dim.4
  86.3 19.8 %all_to_all.20 = bf16[16,256,128]{1,2,0:T(8,128)(2,1)S(1)} all-to-all(bf16[16,256,128]{1,2,0:T(8,128)(2,1)S(1)} %broadcast_in_dim.4), channel_id=1, replica_groups=mesh['ra_0'=4,'ra_1'=4,'cb_0'=16,'cb_1'=2] {'ra_0','ra_1'}, dimensions={0} | all-to-all | bytes 2097152 | tf_op jit(solution)/shard_map/all_to_all | solution.py:54
  106.1 0.3 multiply_reduce_fusion
  106.4 0.3 fusion.1
  106.8 0.0 all-gather.15.cloned.1.call-done
  106.8 2.0 copy.24
  108.8 33.5 %all-gather.11.cloned.1.call-done = bf16[2048,704]{1,0:T(8,128)(2,1)} async-done(((bf16[64,704]{1,0:T(8,128)(2,1)}), bf16[2048,704]{1,0:T(8,128)(2,1)}) %all-gather.11.cloned.1.call-update) | async-done | bytes 2883600 | tf_op jit(solution)/shard_map/all_gather | solution.py:17
  142.3 2.2 fusion.12
  144.5 4.5 %fusion.10 = bf16[32,16,8,128]{3,2,1,0:T(8,128)(2,1)S(1)} fusion(bf16[352,2048]{0,1:T(8,128)(2,1)S(1)} %bitcast.56, bf16[256,2048]{0,1:T(8,128)(2,1)} %copy-done.1, bf16[2048,704]{1,0:T(8,128)(2,1)} %all-gather.11.cloned.1.call-done, f32[256,352]{0,1:T(8,128)S(1)} %fusion.12, f32[352]{0:T(512)S(1)} %copy-done.7), kind=kOutput, calls=%fused_computation.16 | convolution fusion | flops 739352576 | bytes 5473664 | tf_op jit(solution)/shard_map/dot_general | solution.py:80
  149.0 1.3 copy.34
  150.3 6.9 %all-to-all-start.1 = ((bf16[16,256,128]{2,1,0:T(8,128)(2,1)}), bf16[16,256,128]{2,1,0:T(8,128)(2,1)S(1)}, u32[]{:S(2)}, u32[]{:S(2)}) async-start(bf16[16,256,128]{2,1,0:T(8,128)(2,1)} %bitcast.52), calls=%async_computation.1 | async-start | bytes 2097152 | tf_op jit(solution)/shard_map/all_to_all | solution.py:48
  157.1 0.8 dynamic_slice.13
  157.9 0.8 dynamic-slice_multiply_fusion.1
  158.7 16.3 %all-to-all-done.1 = bf16[16,256,128]{2,1,0:T(8,128)(2,1)S(1)} async-done(((bf16[16,256,128]{2,1,0:T(8,128)(2,1)}), bf16[16,256,128]{2,1,0:T(8,128)(2,1)S(1)}, u32[]{:S(2)}, u32[]{:S(2)}) %all-to-all-start.1) | async-done | bytes 1048608 | tf_op jit(solution)/shard_map/all_to_all | solution.py:48
  175.0 0.1 convert_reduce_fusion.1
  175.1 0.1 multiply_reduce_fusion.2
  175.2 8.3 %psum.28 = f32[256]{0:T(256)S(1)} all-reduce(f32[256]{0:T(256)S(1)} %multiply_reduce_fusion.2), channel_id=1, replica_groups=mesh['ra_0'=4,'ra_1'=4,'cb_0'=16,'cb_1'=2] {'ra_0'}, use_global_device_ids=true, to_apply=%region_3.4 | all-reduce | flops 256 | bytes 2048 | tf_op jit(solution)/shard_map/psum | solution.py:63
  183.5 9.1 %psum.29 = f32[256]{0:T(256)S(1)} all-reduce(f32[256]{0:T(256)S(1)} %psum.28), channel_id=1, replica_groups=mesh['ra_0'=4,'ra_1'=4,'cb_0'=16,'cb_1'=2] {'ra_1'}, use_global_device_ids=true, to_apply=%region_4.5 | all-reduce | flops 256 | bytes 2048 | tf_op jit(solution)/shard_map/psum | solution.py:63
  192.7 0.1 multiply_convert_fusion.1
  192.8 0.1 copy.26
  192.9 1.1 broadcast_in_dim.5
  194.0 3.7 %all-to-all-start.2 = ((bf16[16,256,128]{1,2,0:T(8,128)(2,1)}), bf16[16,256,128]{1,2,0:T(8,128)(2,1)S(1)}, u32[]{:S(2)}, u32[]{:S(2)}) async-start(bf16[16,256,128]{1,2,0:T(8,128)(2,1)} %broadcast_in_dim.5), calls=%async_computation.2 | async-start | bytes 2097152 | tf_op jit(solution)/shard_map/all_to_all | solution.py:54
  197.6 0.0 all-gather.17.cloned.1.call-done
  197.7 1.6 copy.27
  199.3 38.3 %all-gather.13.cloned.1.call-done = bf16[2048,704]{1,0:T(8,128)(2,1)} async-done(((bf16[64,704]{1,0:T(8,128)(2,1)}), bf16[2048,704]{1,0:T(8,128)(2,1)}) %all-gather.13.cloned.1.call-update) | async-done | bytes 2883600 | tf_op jit(solution)/shard_map/all_gather | solution.py:17
  237.6 2.2 fusion.18
  239.8 5.2 %fusion.11 = bf16[32,16,8,128]{3,2,1,0:T(8,128)(2,1)} fusion(bf16[352,2048]{0,1:T(8,128)(2,1)S(1)} %bitcast.55, bf16[256,2048]{0,1:T(8,128)(2,1)S(1)} %bitcast.58, bf16[2048,704]{1,0:T(8,128)(2,1)} %all-gather.13.cloned.1.call-done, f32[256,352]{0,1:T(8,128)S(1)} %fusion.18, f32[352]{0:T(512)S(1)} %copy-done.9), kind=kOutput, calls=%fused_computation.17 | convolution fusion | flops 739352576 | bytes 5473664 | tf_op jit(solution)/shard_map/dot_general | solution.py:80
  244.9 2.5 copy.33
  247.4 6.8 %all-to-all-start.3 = ((bf16[16,256,128]{2,1,0:T(8,128)(2,1)}), bf16[16,256,128]{2,1,0:T(8,128)(2,1)S(1)}, u32[]{:S(2)}, u32[]{:S(2)}) async-start(bf16[16,256,128]{2,1,0:T(8,128)(2,1)} %bitcast.50), calls=%async_computation.3 | async-start | bytes 2097152 | tf_op jit(solution)/shard_map/all_to_all | solution.py:48
  254.2 0.8 dynamic_slice.15
  255.0 0.8 dynamic-slice_multiply_fusion
  255.8 16.3 %all-to-all-done.3 = bf16[16,256,128]{2,1,0:T(8,128)(2,1)S(1)} async-done(((bf16[16,256,128]{2,1,0:T(8,128)(2,1)}), bf16[16,256,128]{2,1,0:T(8,128)(2,1)S(1)}, u32[]{:S(2)}, u32[]{:S(2)}) %all-to-all-start.3) | async-done | bytes 1048608 | tf_op jit(solution)/shard_map/all_to_all | solution.py:48
  272.1 0.1 convert_reduce_fusion
  272.2 0.1 multiply_reduce_fusion.1
  272.3 8.3 %psum.30 = f32[256]{0:T(256)S(1)} all-reduce(f32[256]{0:T(256)S(1)} %multiply_reduce_fusion.1), channel_id=1, replica_groups=mesh['ra_0'=4,'ra_1'=4,'cb_0'=16,'cb_1'=2] {'ra_0'}, use_global_device_ids=true, to_apply=%region_7.8 | all-reduce | flops 256 | bytes 2048 | tf_op jit(solution)/shard_map/psum | solution.py:63
  280.6 9.1 %psum.31 = f32[256]{0:T(256)S(1)} all-reduce(f32[256]{0:T(256)S(1)} %psum.30), channel_id=1, replica_groups=mesh['ra_0'=4,'ra_1'=4,'cb_0'=16,'cb_1'=2] {'ra_1'}, use_global_device_ids=true, to_apply=%region_8.9 | all-reduce | flops 256 | bytes 2048 | tf_op jit(solution)/shard_map/psum | solution.py:63
  289.8 0.7 multiply_convert_fusion
  (32 shorter events, 0.2 us)
Async XLA Ops:
  6.5 44.6 %copy-start.2 = (f32[352,64]{0,1:T(8,128)S(1)}, f32[352,64]{0,1:T(8,128)}, u32[]{:S(2)}) copy-start(f32[352,64]{0,1:T(8,128)} %param.29) | copy-start | bytes 270340
  6.5 78.7 %copy-start.3 = (f32[64,352]{1,0:T(8,128)S(1)}, f32[64,352]{1,0:T(8,128)}, u32[]{:S(2)}) copy-start(f32[64,352]{1,0:T(8,128)} %param.25) | copy-start | bytes 270340
  6.5 100.3 %all-gather.15.cloned.1.call-start = ((), (), s32[]{:S(2)}) async-start(), calls=%async_computation.6 | async-start | bytes 2359296 | tf_op jit(solution)/shard_map/all_gather | solution.py:30
  7.5 77.8 %copy-start.4 = (f32[64,352]{1,0:T(8,128)S(1)}, f32[64,352]{1,0:T(8,128)}, u32[]{:S(2)}) copy-start(f32[64,352]{1,0:T(8,128)} %param.27) | copy-start | bytes 270340
  7.5 78.6 %copy-start = (bf16[256,128]{1,0:T(8,128)(2,1)S(1)}, bf16[256,128]{1,0:T(8,128)(2,1)}, u32[]{:S(2)}) copy-start(bf16[256,128]{1,0:T(8,128)(2,1)} %param.16) | copy-start | bytes 196612
  48.5 93.8 %all-gather.11.cloned.1.call-start = ((), (), s32[]{:S(2)}) async-start(), calls=%async_computation.4 | async-start | bytes 3244032 | tf_op jit(solution)/shard_map/all_gather | solution.py:17
  51.1 146.6 %all-gather.17.cloned.1.call-start = ((), (), s32[]{:S(2)}) async-start(), calls=%async_computation.7 | async-start | bytes 2359296 | tf_op jit(solution)/shard_map/all_gather | solution.py:30
  85.2 152.4 %all-gather.13.cloned.1.call-start = ((), (), s32[]{:S(2)}) async-start(), calls=%async_computation.5 | async-start | bytes 3244032 | tf_op jit(solution)/shard_map/all_gather | solution.py:17
  86.2 20.3 %copy-start.5 = (f32[2048]{0:T(1024)S(1)}, f32[2048]{0:T(1024)}, u32[]{:S(2)}) copy-start(f32[2048]{0:T(1024)} %param.17) | copy-start | bytes 24580
  106.8 37.7 %copy-start.1 = (bf16[256,2048]{0,1:T(8,128)(2,1)}, bf16[256,2048]{0,1:T(8,128)(2,1)S(1)}, u32[]{:S(2)}) copy-start(bf16[256,2048]{0,1:T(8,128)(2,1)S(1)} %fusion.1) | copy-start | bytes 3145732
  106.8 35.5 %copy-start.6 = (f32[352]{0:T(512)S(1)}, f32[352]{0:T(512)}, u32[]{:S(2)}) copy-start(f32[352]{0:T(512)} %param.19) | copy-start | bytes 4228
  108.8 35.7 %copy-start.7 = (f32[352]{0:T(512)S(1)}, f32[352]{0:T(512)}, u32[]{:S(2)}) copy-start(f32[352]{0:T(512)} %param.21) | copy-start | bytes 4228
  150.3 24.7 %all-to-all-start.1 = ((bf16[16,256,128]{2,1,0:T(8,128)(2,1)}), bf16[16,256,128]{2,1,0:T(8,128)(2,1)S(1)}, u32[]{:S(2)}, u32[]{:S(2)}) async-start(bf16[16,256,128]{2,1,0:T(8,128)(2,1)} %bitcast.52), calls=%async_computation.1 | async-start | bytes 2097152 | tf_op jit(solution)/shard_map/all_to_all | solution.py:48
  194.0 43.6 %all-to-all-start.2 = ((bf16[16,256,128]{1,2,0:T(8,128)(2,1)}), bf16[16,256,128]{1,2,0:T(8,128)(2,1)S(1)}, u32[]{:S(2)}, u32[]{:S(2)}) async-start(bf16[16,256,128]{1,2,0:T(8,128)(2,1)} %broadcast_in_dim.5), calls=%async_computation.2 | async-start | bytes 2097152 | tf_op jit(solution)/shard_map/all_to_all | solution.py:54
  197.6 39.9 %copy-start.8 = (f32[352]{0:T(512)S(1)}, f32[352]{0:T(512)}, u32[]{:S(2)}) copy-start(f32[352]{0:T(512)} %param.26) | copy-start | bytes 4228
  199.3 40.5 %copy-start.9 = (f32[352]{0:T(512)S(1)}, f32[352]{0:T(512)}, u32[]{:S(2)}) copy-start(f32[352]{0:T(512)} %param.28) | copy-start | bytes 4228
  247.4 24.7 %all-to-all-start.3 = ((bf16[16,256,128]{2,1,0:T(8,128)(2,1)}), bf16[16,256,128]{2,1,0:T(8,128)(2,1)S(1)}, u32[]{:S(2)}, u32[]{:S(2)}) async-start(bf16[16,256,128]{2,1,0:T(8,128)(2,1)} %bitcast.50), calls=%async_computation.3 | async-start | bytes 2097152 | tf_op jit(solution)/shard_map/all_to_all | solution.py:48
Sparse Core Ops, SparseCore 0:
  48.6 17.6 all-gather.14
  68.4 73.8 all-gather.10
  144.4 17.3 all-gather.16
  163.8 73.7 all-gather.12
where the time goes:
time: 298 us; the launch traced here: 297 us
  blocking collectives  130 us (44%)
  waiting for transfers between devices  105 us (35%)
  starting transfers between devices  17.5 us (6%)
  matrix products  14 us (5%)
  between operations  13.4 us (4%)
  local copies, waits for them, and re-layouts  10.2 us (3%)
  other arithmetic  7.79 us (3%)
    all_gather x2, blocking collectives, all_blocks(): pieces = lax.all_gather(pieces, axes[k])  75 us
    all_gather x2, waiting for transfers between devices, in_one_piece(): out = lax.all_gather(both, axis, axis=dim, tiled=True)  71.8 us
    psum x4, blocking collectives, by_axis(): return functools.reduce(lax.psum, axes, x)  34.8 us
    all_to_all x2, waiting for transfers between devices, sent_and_summed(): lax.all_to_all(pieces, axis, split_axis=0, concat_axis=0, tiled=True)  32.6 us
    all_to_all x1, blocking collectives, copy_for_each(): return lax.all_to_all(copies, axis, split_axis=0, concat_axis=0, tiled=True)  19.8 us
    all_to_all x2, starting transfers between devices, sent_and_summed(): lax.all_to_all(pieces, axis, split_axis=0, concat_axis=0, tiled=True)  13.7 us
    dot_general x2, matrix products, expand(): jnp.dot(hidden, gather_axes(w_down.astype(jnp.bfloat16), CB, (0, 1), 1),...  9.67 us
  transfers between devices with their start and end apart: 7, of which 4 were waited for; matrix products, arithmetic and copies ran while one was open for 7% of the time, Pallas kernels for 0%

commit v1 on v0

v1 whole, which is shorter than its diff:
```python
import functools

import jax
import jax.numpy as jnp
from jax import lax
from jax.experimental import pallas as pl
from jax.experimental.pallas import tpu as pltpu
from jax.sharding import Mesh
from jax.sharding import PartitionSpec as P

D = 2048
RA = ("ra_0", "ra_1")
CB = ("cb_0", "cb_1")
LANES = 384
EPS = 1e-06


def pack_body(g1, u1, d1, g2, u2, d2, out):
    rows, width = g1.shape

    def put(at, value):
        out[:, at : at + LANES] = jnp.zeros((rows, LANES), jnp.bfloat16)
        out[:, at : at + width] = value.astype(jnp.bfloat16)

    put(0, g1[...])
    put(LANES, u1[...])
    put(2 * LANES, g2[...])
    put(3 * LANES, u2[...])
    put(4 * LANES, d1[...].T)
    put(5 * LANES, d2[...].T)


def pack(g1, u1, d1, g2, u2, d2):
    rows = g1.shape[0]
    return pl.pallas_call(
        pack_body,
        out_shape=jax.ShapeDtypeStruct((rows, 6 * LANES), jnp.bfloat16),
    )(g1, u1, d1, g2, u2, d2)


def block_body(steps, first, x, gain, w_in, w_down, s_gate, s_up, out, normed, gate_up, hidden):
    k = pl.program_id(0)
    chunk = w_in.shape[0]

    @pl.when(k == 0)
    def _():
        gate_up[...] = jnp.zeros_like(gate_up)
        if first:
            count = x.shape[0]
            total = jnp.zeros((x.shape[1], 1), jnp.float32)
            for j in range(count):
                piece = x[j].astype(jnp.float32)
                total += jnp.sum(piece * piece, axis=1, keepdims=True)
            scale = lax.rsqrt(total / D + EPS)
            for j in range(count):
                at = slice(j * x.shape[2], (j + 1) * x.shape[2])
                value = x[j].astype(jnp.float32) * scale * gain[:, at]
                normed[:, at] = value.astype(jnp.bfloat16)

    source = normed if first else x

    @pl.when(k < steps)
    def _():
        at = pl.multiple_of(k * chunk, chunk)
        gate_up[...] += jnp.dot(
            source[:, pl.ds(at, chunk)], w_in[...], preferred_element_type=jnp.float32
        )

    @pl.when(k == steps - 1)
    def _():
        gate = gate_up[:, :LANES] * s_gate[...]
        upper = gate_up[:, LANES:] * s_up[...]
        hidden[...] = (gate / (1.0 + jnp.exp(-gate)) * upper).astype(jnp.bfloat16)

    @pl.when(k >= steps)
    def _():
        out[...] = lax.dot_general(
            hidden[...],
            w_down[...],
            (((1,), (1,)), ((), ())),
            preferred_element_type=jnp.float32,
        ).astype(jnp.bfloat16)


def block(x, gain, weights, which, s_gate, s_up, steps=4):
    first = x.ndim == 3
    rows = x.shape[1] if first else x.shape[0]
    chunk = D // steps
    return pl.pallas_call(
        functools.partial(block_body, steps, first),
        grid=(2 * steps,),
        in_specs=[
            pl.BlockSpec(x.shape, lambda k: (0,) * x.ndim),
            pl.BlockSpec((1, D), lambda k: (0, 0)),
            pl.BlockSpec((chunk, 2 * LANES), lambda k: (jnp.minimum(k, steps - 1), which)),
            pl.BlockSpec((chunk, LANES), lambda k: (jnp.maximum(k - steps, 0), 4 + which)),
            pl.BlockSpec((1, LANES), lambda k: (0, 0)),
            pl.BlockSpec((1, LANES), lambda k: (0, 0)),
        ],
        out_specs=pl.BlockSpec((rows, chunk), lambda k: (0, jnp.maximum(k - steps, 0))),
        out_shape=jax.ShapeDtypeStruct((rows, D), jnp.bfloat16),
        scratch_shapes=[
            pltpu.VMEM((rows, D) if first else (8, 128), jnp.bfloat16),
            pltpu.VMEM((rows, 2 * LANES), jnp.float32),
            pltpu.VMEM((rows, LANES), jnp.bfloat16),
        ],
    )(x, gain, weights, weights, s_gate, s_up)


def exchange(pieces):
    return lax.all_to_all(pieces, RA, split_axis=0, concat_axis=0, tiled=True)


def copy_for_each(x):
    return exchange(jnp.broadcast_to(x, (lax.axis_size(RA), *x.shape)))


def by_rows(partial_value):
    pieces = partial_value.reshape(lax.axis_size(RA), -1, D)
    return exchange(pieces).astype(jnp.float32).sum(axis=0)


def normalized(values, gain):
    meansq = jnp.mean(values * values, axis=1, keepdims=True)
    return (values * lax.rsqrt(meansq + EPS) * gain).astype(jnp.bfloat16)


def padded(scale):
    return jnp.pad(scale, (0, LANES - scale.shape[0]))[None]


def shards(
    tokens,
    gain_first,
    gate_first,
    gate_first_scale,
    up_first,
    up_first_scale,
    down_first,
    down_first_scale,
    gain_second,
    gate_second,
    gate_second_scale,
    up_second,
    up_second_scale,
    down_second,
    down_second_scale,
    gain_last,
):
    count = lax.axis_size(RA)
    packed = pack(gate_first, up_first, down_first, gate_second, up_second, down_second)
    weights = lax.all_gather(packed, CB, axis=0, tiled=True)
    pieces = copy_for_each(tokens)
    rows = tokens.shape[0] // count
    own = lax.dynamic_slice_in_dim(pieces, lax.axis_index(RA) * rows, rows, 1)
    own = jnp.moveaxis(own, 0, 1).reshape(rows, D).astype(jnp.float32)
    partial_first = block(
        pieces, gain_first[None], weights, 0, padded(gate_first_scale), padded(up_first_scale)
    )
    first = 0.1 * own + 0.5 * by_rows(partial_first) * down_first_scale
    normed = copy_for_each(normalized(first, gain_second)).reshape(-1, D)
    partial_second = block(
        normed, gain_second[None], weights, 1, padded(gate_second_scale), padded(up_second_scale)
    )
    second = 0.1 * first + 0.5 * by_rows(partial_second) * down_second_scale
    mixed = normalized(second, gain_last)
    columns = jnp.moveaxis(mixed.reshape(rows, count, -1), 1, 0)
    return exchange(columns).reshape(tokens.shape)


def solution(mesh):
    torus = Mesh(mesh.devices.reshape(4, 4, 16, 2), ("ra_0", "ra_1", "cb_0", "cb_1"))
    weight, across = P(CB, RA), P(RA, CB)
    return jax.shard_map(
        shards,
        mesh=torus,
        in_specs=(
            P(CB, RA),
            P(),
            weight,
            P(RA),
            weight,
            P(RA),
            across,
            P(),
            P(),
            weight,
            P(RA),
            weight,
            P(RA),
            across,
            P(),
            P(),
        ),
        out_specs=P(CB, RA),
        check_vma=False,
    )
```

time: 298 us -> 204 us (0.68)
  the two profiles are of different devices: /device:TPU:32 before, /device:TPU:2 now
where the time goes in v1:
time: 204 us; the launch traced here: 203 us
  waiting for transfers between devices  118 us (58%)
  starting transfers between devices  27.4 us (13%)
  Pallas kernels  18.5 us (9%)
  between operations  13.5 us (7%)
  blocking collectives  10.6 us (5%)
  local copies, waits for them, and re-layouts  10.4 us (5%)
  other arithmetic  4.2 us (2%)
    all_to_all x4, waiting for transfers between devices, exchange(): return lax.all_to_all(pieces, RA, split_axis=0, concat_axis=0, tiled=True)  59.1 us
    all_gather x1, waiting for transfers between devices, shards(): weights = lax.all_gather(packed, CB, axis=0, tiled=True)  58.8 us
    all_to_all x4, starting transfers between devices, exchange(): return lax.all_to_all(pieces, RA, split_axis=0, concat_axis=0, tiled=True)  27.4 us
    pallas_call x2, Pallas kernels, block(): pl.pallas_call(functools.partial(block_body, steps, first), grid=(2 * ste...  16.5 us
    all_to_all x1, blocking collectives, exchange(): return lax.all_to_all(pieces, RA, split_axis=0, concat_axis=0, tiled=True)  10.6 us
    unnamed x23, local copies, waits for them, and re-layouts  5.02 us
  transfers between devices with their start and end apart: 5, of which 5 were waited for; matrix products, arithmetic and copies ran while one was open for 2% of the time, Pallas kernels for 0%

profile of v1, /device:TPU:2, one launch (start us, length us, event | category | flops | bytes accessed | tf_op | source)
XLA Modules:
  0.0 202.5 jit_solution(4994158679687661175)
XLA Ops:
  6.5 0.0 all-gather.2.cloned.1.call-start
  6.5 1.7 copy.21.d1
  8.2 1.7 copy.22.d2
  9.9 0.0 copy-start.6
  9.9 0.0 copy-start.7
  9.9 2.1 %shard_map.154 = bf16[64,2304]{1,0:T(8,128)(2,1)} custom-call(f32[64,352]{1,0:T(8,128)} %g1.1, f32[64,352]{1,0:T(8,128)} %u1_.1, f32[352,64]{1,0:T(8,128)} %copy.21.d1, f32[64,352]{1,0:T(8,128)} %g2.1, f32[64,352]{1,0:T(8,128)} %u2_.1, f32[352,64]{1,0:T(8,128)} %copy.22.d2), custom_call_target="tpu_custom_call" | custom-call | tf_op jit(solution)/shard_map/pallas_call | solution.py:35
  12.0 0.0 all-gather.2.cloned.1.call-update
  12.0 2.0 broadcast_in_dim.30
  14.0 9.3 %all-to-all-start = ((bf16[16,256,128]{2,1,0:T(8,128)(2,1)}), bf16[16,256,128]{2,1,0:T(8,128)(2,1)S(1)}, u32[]{:S(2)}, u32[]{:S(2)}) async-start(bf16[16,256,128]{2,1,0:T(8,128)(2,1)} %broadcast_in_dim.30), calls=%async_computation | async-start | bytes 2097152 | tf_op jit(solution)/shard_map/all_to_all | solution.py:111
  23.3 0.0 copy-done.6
  23.3 0.6 broadcast_in_dim.32.s_gate
  23.9 0.0 copy-done.7
  23.9 0.6 broadcast_in_dim.33.s_up
  24.5 13.2 %all-to-all-done.x = bf16[16,256,128]{2,1,0:T(8,128)(2,1)S(1)} async-done(((bf16[16,256,128]{2,1,0:T(8,128)(2,1)}), bf16[16,256,128]{2,1,0:T(8,128)(2,1)S(1)}, u32[]{:S(2)}, u32[]{:S(2)}) %all-to-all-start) | async-done | bytes 1048608 | tf_op jit(solution)/shard_map/all_to_all | solution.py:111
  37.7 0.0 copy-start
  37.7 58.8 %all-gather.2.cloned.1.call-done.w_in.w_down = bf16[2048,2304]{1,0:T(8,128)(2,1)} async-done(((bf16[64,2304]{1,0:T(8,128)(2,1)}), bf16[2048,2304]{1,0:T(8,128)(2,1)}) %all-gather.2.cloned.1.call-update) | async-done | bytes 9437200 | tf_op jit(solution)/shard_map/all_gather | solution.py:152
  96.5 0.0 copy-done
  96.5 8.7 %shard_map.155 = bf16[256,2048]{1,0:T(8,128)(2,1)} custom-call(bf16[16,256,128]{2,1,0:T(8,128)(2,1)} %copy-done, f32[1,2048]{1,0:T(1,128)} %bitcast.71, bf16[2048,2304]{1,0:T(8,128)(2,1)} %all-gather.2.cloned.1.call-done.w_in.w_down, bf16[2048,2304]{1,0:T(8,128)(2,1)} %all-gather.2.cloned.1.call-done.w_in.w_down, f32[1,384]{1,0:T(1,128)} %broadcast_in_dim.32.s_gate, ...), custom_call_target="tpu_custom_call" | custom-call | tf_op jit(solution)/shard_map/pallas_call | solution.py:89
  105.2 0.0 copy-start.3
  105.2 0.0 copy-start.2
  105.2 7.4 %all-to-all-start.1 = ((bf16[16,16,2048]{2,1,0:T(8,128)(2,1)}), bf16[16,16,2048]{2,1,0:T(8,128)(2,1)S(1)}, u32[]{:S(2)}, u32[]{:S(2)}) async-start(bf16[16,16,2048]{2,1,0:T(8,128)(2,1)} %bitcast.66), calls=%async_computation.1 | async-start | bytes 2097152 | tf_op jit(solution)/shard_map/all_to_all | solution.py:111
  112.6 0.0 copy-done.3
  112.6 16.2 %all-to-all-done.1 = bf16[16,16,2048]{2,1,0:T(8,128)(2,1)S(1)} async-done(((bf16[16,16,2048]{2,1,0:T(8,128)(2,1)}), bf16[16,16,2048]{2,1,0:T(8,128)(2,1)S(1)}, u32[]{:S(2)}, u32[]{:S(2)}) %all-to-all-start.1) | async-done | bytes 1048608 | tf_op jit(solution)/shard_map/all_to_all | solution.py:111
  128.7 0.1 convert_reduce_fusion.1
  128.9 0.0 copy-start.8
  128.9 0.0 copy-start.9
  128.9 1.0 multiply_reduce_fusion.1
  129.9 0.0 copy-done.2
  129.9 0.9 fusion.2
  130.9 1.1 broadcast_in_dim.34
  132.0 5.2 %all-to-all-start.2 = ((bf16[16,16,2048]{2,1,0:T(8,128)(2,1)}), bf16[16,16,2048]{2,1,0:T(8,128)(2,1)S(1)}, u32[]{:S(2)}, u32[]{:S(2)}) async-start(bf16[16,16,2048]{2,1,0:T(8,128)(2,1)} %broadcast_in_dim.34), calls=%async_computation.2 | async-start | bytes 2097152 | tf_op jit(solution)/shard_map/all_to_all | solution.py:111
  137.2 0.0 copy-done.8
  137.2 0.6 broadcast_in_dim.36.s_gate
  137.7 0.0 copy-done.9
  137.8 0.5 broadcast_in_dim.37.s_up
  138.3 14.7 %all-to-all-done.2 = bf16[16,16,2048]{2,1,0:T(8,128)(2,1)S(1)} async-done(((bf16[16,16,2048]{2,1,0:T(8,128)(2,1)}), bf16[16,16,2048]{2,1,0:T(8,128)(2,1)S(1)}, u32[]{:S(2)}, u32[]{:S(2)}) %all-to-all-start.2) | async-done | bytes 1048608 | tf_op jit(solution)/shard_map/all_to_all | solution.py:111
  153.0 0.0 copy-start.1
  153.0 1.0 copy-done.1
  153.9 7.8 %shard_map.156 = bf16[256,2048]{1,0:T(8,128)(2,1)} custom-call(bf16[256,2048]{1,0:T(8,128)(2,1)} %bitcast.67, f32[1,2048]{1,0:T(1,128)} %bitcast.70, bf16[2048,2304]{1,0:T(8,128)(2,1)} %all-gather.2.cloned.1.call-done.w_in.w_down, bf16[2048,2304]{1,0:T(8,128)(2,1)} %all-gather.2.cloned.1.call-done.w_in.w_down, f32[1,384]{1,0:T(1,128)} %broadcast_in_dim.36.s_gate, ...), custom_call_target="tpu_custom_call" | custom-call | tf_op jit(solution)/shard_map/pallas_call | solution.py:89
  161.7 5.5 %all-to-all-start.3 = ((bf16[16,16,2048]{2,1,0:T(8,128)(2,1)}), bf16[16,16,2048]{2,1,0:T(8,128)(2,1)S(1)}, u32[]{:S(2)}, u32[]{:S(2)}) async-start(bf16[16,16,2048]{2,1,0:T(8,128)(2,1)} %bitcast.68), calls=%async_computation.3 | async-start | bytes 2097152 | tf_op jit(solution)/shard_map/all_to_all | solution.py:111
  167.2 0.0 copy-done.5
  167.3 15.1 %all-to-all-done.3 = bf16[16,16,2048]{2,1,0:T(8,128)(2,1)S(1)} async-done(((bf16[16,16,2048]{2,1,0:T(8,128)(2,1)}), bf16[16,16,2048]{2,1,0:T(8,128)(2,1)S(1)}, u32[]{:S(2)}, u32[]{:S(2)}) %all-to-all-start.3) | async-done | bytes 1048608 | tf_op jit(solution)/shard_map/all_to_all | solution.py:111
  182.4 0.1 convert_reduce_fusion
  182.5 1.0 multiply_reduce_fusion
  183.5 0.0 copy-done.4
  183.5 0.9 fusion.6
  184.5 10.6 %all_to_all.25 = bf16[16,16,128]{2,1,0:T(8,128)(2,1)S(1)} all-to-all(bf16[16,16,128]{2,1,0:T(8,128)(2,1)S(1)} %fusion.6), channel_id=1, replica_groups=mesh['ra_0'=4,'ra_1'=4,'cb_0'=16,'cb_1'=2] {'ra_0','ra_1'}, dimensions={0} | all-to-all | bytes 131072 | tf_op jit(solution)/shard_map/all_to_all | solution.py:111
  195.1 0.6 copy.45
  (10 shorter events, 0.0 us)
Async XLA Ops:
  6.5 90.0 %all-gather.2.cloned.1.call-start = ((), (), s32[]{:S(2)}) async-start(), calls=%async_computation.5 | async-start | bytes 9732096 | tf_op jit(solution)/shard_map/all_gather | solution.py:152
  9.9 13.4 %copy-start.6 = (f32[352]{0:T(512)S(1)}, f32[352]{0:T(512)}, u32[]{:S(2)}) copy-start(f32[352]{0:T(512)} %param.19) | copy-start | bytes 4228
  9.9 14.0 %copy-start.7 = (f32[352]{0:T(512)S(1)}, f32[352]{0:T(512)}, u32[]{:S(2)}) copy-start(f32[352]{0:T(512)} %param.21) | copy-start | bytes 4228
  14.0 23.7 %all-to-all-start = ((bf16[16,256,128]{2,1,0:T(8,128)(2,1)}), bf16[16,256,128]{2,1,0:T(8,128)(2,1)S(1)}, u32[]{:S(2)}, u32[]{:S(2)}) async-start(bf16[16,256,128]{2,1,0:T(8,128)(2,1)} %broadcast_in_dim.30), calls=%async_computation | async-start | bytes 2097152 | tf_op jit(solution)/shard_map/all_to_all | solution.py:111
  37.7 58.8 %copy-start = (bf16[16,256,128]{2,1,0:T(8,128)(2,1)}, bf16[16,256,128]{2,1,0:T(8,128)(2,1)S(1)}, u32[]{:S(2)}) copy-start(bf16[16,256,128]{2,1,0:T(8,128)(2,1)S(1)} %all-to-all-done.x) | copy-start | bytes 3145732
  105.2 7.4 %copy-start.3 = (f32[2048]{0:T(1024)S(1)}, f32[2048]{0:T(1024)}, u32[]{:S(2)}) copy-start(f32[2048]{0:T(1024)} %param.23) | copy-start | bytes 24580
  105.2 24.7 %copy-start.2 = (f32[2048]{0:T(1024)S(1)}, f32[2048]{0:T(1024)}, u32[]{:S(2)}) copy-start(f32[2048]{0:T(1024)} %param.24) | copy-start | bytes 24580
  105.2 23.5 %all-to-all-start.1 = ((bf16[16,16,2048]{2,1,0:T(8,128)(2,1)}), bf16[16,16,2048]{2,1,0:T(8,128)(2,1)S(1)}, u32[]{:S(2)}, u32[]{:S(2)}) async-start(bf16[16,16,2048]{2,1,0:T(8,128)(2,1)} %bitcast.66), calls=%async_computation.1 | async-start | bytes 2097152 | tf_op jit(solution)/shard_map/all_to_all | solution.py:111
  128.9 8.3 %copy-start.8 = (f32[352]{0:T(512)S(1)}, f32[352]{0:T(512)}, u32[]{:S(2)}) copy-start(f32[352]{0:T(512)} %param.26) | copy-start | bytes 4228
  128.9 8.9 %copy-start.9 = (f32[352]{0:T(512)S(1)}, f32[352]{0:T(512)}, u32[]{:S(2)}) copy-start(f32[352]{0:T(512)} %param.28) | copy-start | bytes 4228
  132.0 21.0 %all-to-all-start.2 = ((bf16[16,16,2048]{2,1,0:T(8,128)(2,1)}), bf16[16,16,2048]{2,1,0:T(8,128)(2,1)S(1)}, u32[]{:S(2)}, u32[]{:S(2)}) async-start(bf16[16,16,2048]{2,1,0:T(8,128)(2,1)} %broadcast_in_dim.34), calls=%async_computation.2 | async-start | bytes 2097152 | tf_op jit(solution)/shard_map/all_to_all | solution.py:111
  153.0 1.0 copy-start.1
  161.7 5.5 %copy-start.5 = (f32[2048]{0:T(1024)S(1)}, f32[2048]{0:T(1024)}, u32[]{:S(2)}) copy-start(f32[2048]{0:T(1024)} %param.30) | copy-start | bytes 24580
  161.7 21.8 %copy-start.4 = (f32[2048]{0:T(1024)S(1)}, f32[2048]{0:T(1024)}, u32[]{:S(2)}) copy-start(f32[2048]{0:T(1024)} %param.31) | copy-start | bytes 24580
  161.7 20.6 %all-to-all-start.3 = ((bf16[16,16,2048]{2,1,0:T(8,128)(2,1)}), bf16[16,16,2048]{2,1,0:T(8,128)(2,1)S(1)}, u32[]{:S(2)}, u32[]{:S(2)}) async-start(bf16[16,16,2048]{2,1,0:T(8,128)(2,1)} %bitcast.68), calls=%async_computation.3 | async-start | bytes 2097152 | tf_op jit(solution)/shard_map/all_to_all | solution.py:111
Sparse Core Ops, SparseCore 0:
  12.1 84.3 all-gather.1

commit v2 on v1

v2 whole, which is shorter than its diff:
```python
import functools

import jax
import jax.numpy as jnp
from jax import lax
from jax.experimental import pallas as pl
from jax.experimental.pallas import tpu as pltpu
from jax.sharding import Mesh
from jax.sharding import PartitionSpec as P

D = 2048
RA = ("ra_0", "ra_1")
CB = ("cb_0", "cb_1")
LANES = 384
EPS = 1e-06
LIFT = 2.0**18
ROOM = pltpu.CompilerParams(vmem_limit_bytes=20 * 1024 * 1024)


def pack_body(g1, u1, d1, g2, u2, d2, out):
    rows, width = g1.shape
    out[...] = jnp.zeros_like(out)
    for j, piece in enumerate((g1, u1, d1, g2, u2, d2)):
        out[:, j * LANES : j * LANES + width] = piece[...].astype(jnp.bfloat16) * LIFT


def pack(g1, u1, d1, g2, u2, d2):
    rows = g1.shape[0]
    return pl.pallas_call(
        pack_body,
        out_shape=jax.ShapeDtypeStruct((rows, 6 * LANES), jnp.bfloat16),
        compiler_params=ROOM,
    )(g1, u1, d1.T, g2, u2, d2.T)


def spread_body(pieces, gain, out):
    count, rows, width = pieces.shape
    total = jnp.zeros((rows, 1), jnp.float32)
    for j in range(count):
        piece = pieces[j].astype(jnp.float32)
        total += jnp.sum(piece * piece, axis=1, keepdims=True)
    scale = lax.rsqrt(total / D + EPS)
    for j in range(count):
        at = slice(j * width, (j + 1) * width)
        out[:, at] = (pieces[j].astype(jnp.float32) * scale * gain[:, at]).astype(jnp.bfloat16)


def spread(pieces, gain):
    return pl.pallas_call(
        spread_body,
        out_shape=jax.ShapeDtypeStruct((pieces.shape[1], D), jnp.bfloat16),
        compiler_params=ROOM,
    )(pieces, gain[None])


def block_body(x, weights, s_gate, s_up, out):
    both = jnp.dot(x[...], weights[:, : 2 * LANES], preferred_element_type=jnp.float32)
    gate = both[:, :LANES] * s_gate[...]
    upper = both[:, LANES:] * s_up[...]
    hidden = (gate / (1.0 + jnp.exp(-gate)) * upper).astype(jnp.bfloat16)
    out[...] = lax.dot_general(
        hidden,
        weights[:, 2 * LANES :],
        (((1,), (1,)), ((), ())),
        preferred_element_type=jnp.float32,
    ).astype(jnp.bfloat16)


def block(x, weights, s_gate, s_up):
    return pl.pallas_call(
        block_body,
        out_shape=jax.ShapeDtypeStruct(x.shape, jnp.bfloat16),
        compiler_params=ROOM,
    )(x, weights, s_gate, s_up)


def join_body(pieces, before, scale, gain, total, out):
    count = pieces.shape[0]
    added = pieces[0].astype(jnp.float32)
    for j in range(1, count):
        added += pieces[j].astype(jnp.float32)
    values = 0.1 * before[...] + (0.5 / LIFT) * added * scale[...]
    total[...] = values
    meansq = jnp.sum(values * values, axis=1, keepdims=True) / D
    normed = (values * lax.rsqrt(meansq + EPS) * gain[...]).astype(jnp.bfloat16)
    if len(out.shape) == 3:
        for j in range(count):
            out[j] = normed
    else:
        out[...] = normed


def join(pieces, before, scale, gain, copies):
    count, rows, _ = pieces.shape
    shape = (count, rows, D) if copies else (rows, D)
    return pl.pallas_call(
        join_body,
        out_shape=(
            jax.ShapeDtypeStruct((rows, D), jnp.float32),
            jax.ShapeDtypeStruct(shape, jnp.bfloat16),
        ),
        compiler_params=ROOM,
    )(pieces, before, scale[None], gain[None])


def exchange(pieces):
    return lax.all_to_all(pieces, RA, split_axis=0, concat_axis=0, tiled=True)


def copy_for_each(x):
    return exchange(jnp.broadcast_to(x, (lax.axis_size(RA), *x.shape)))


def by_rows(partial_value):
    return exchange(partial_value.reshape(lax.axis_size(RA), -1, D))


def padded(scale):
    return jnp.pad(scale / LIFT, (0, LANES - scale.shape[0]))[None]


def shards(
    tokens,
    gain_first,
    gate_first,
    gate_first_scale,
    up_first,
    up_first_scale,
    down_first,
    down_first_scale,
    gain_second,
    gate_second,
    gate_second_scale,
    up_second,
    up_second_scale,
    down_second,
    down_second_scale,
    gain_last,
):
    count = lax.axis_size(RA)
    packed = pack(gate_first, up_first, down_first, gate_second, up_second, down_second)
    pieces = copy_for_each(tokens)
    weights = lax.all_gather(packed.astype(jnp.float16), CB, axis=0, tiled=True)
    rows = tokens.shape[0] // count
    normed = spread(pieces, gain_first)
    own = lax.dynamic_slice_in_dim(pieces, lax.axis_index(RA) * rows, rows, 1)
    own = jnp.moveaxis(own, 0, 1).reshape(rows, D).astype(jnp.float32)
    w_first, w_second = (w.astype(jnp.bfloat16) for w in jnp.split(weights, 2, axis=1))
    partial_first = block(normed, w_first, padded(gate_first_scale), padded(up_first_scale))
    first, copies = join(by_rows(partial_first), own, down_first_scale, gain_second, True)
    normed = exchange(copies).reshape(-1, D)
    partial_second = block(normed, w_second, padded(gate_second_scale), padded(up_second_scale))
    _, mixed = join(by_rows(partial_second), first, down_second_scale, gain_last, False)
    columns = jnp.moveaxis(mixed.reshape(rows, count, -1), 1, 0)
    return exchange(columns).reshape(tokens.shape)


def solution(mesh):
    torus = Mesh(mesh.devices.reshape(4, 4, 16, 2), ("ra_0", "ra_1", "cb_0", "cb_1"))
    weight, across = P(CB, RA), P(RA, CB)
    return jax.shard_map(
        shards,
        mesh=torus,
        in_specs=(
            P(CB, RA),
            P(),
            weight,
            P(RA),
            weight,
            P(RA),
            across,
            P(),
            P(),
            weight,
            P(RA),
            weight,
            P(RA),
            across,
            P(),
            P(),
        ),
        out_specs=P(CB, RA),
        check_vma=False,
    )
```

time: 204 us -> 186 us (0.912)
  the two profiles are of different devices: /device:TPU:2 before, /device:TPU:32 now
where the time goes in v2:
time: 186 us
  blocking collectives  102 us (55%)
  waiting for transfers between devices  35.5 us (19%)
  starting transfers between devices  17.8 us (10%)
  local copies, waits for them, and re-layouts  12.8 us (7%)
  other arithmetic  9.01 us (5%)
  Pallas kernels  8.34 us (4%)
    all_gather x1, blocking collectives, shards(): weights = lax.all_gather(packed.astype(jnp.float16), CB, axis=0, tiled=True)  71.9 us
    all_to_all x3, waiting for transfers between devices, exchange(): return lax.all_to_all(pieces, RA, split_axis=0, concat_axis=0, tiled=True)  35.5 us
    all_to_all x2, blocking collectives, exchange(): return lax.all_to_all(pieces, RA, split_axis=0, concat_axis=0, tiled=True)  30 us
    all_to_all x3, starting transfers between devices, exchange(): return lax.all_to_all(pieces, RA, split_axis=0, concat_axis=0, tiled=True)  17.8 us
    unnamed x35, local copies, waits for them, and re-layouts  10.7 us
    convert_element_type x1, other arithmetic, shards(): w.astype(jnp.bfloat16)  8.93 us
    pallas_call x2, Pallas kernels, block(): pl.pallas_call(block_body, out_shape=jax.ShapeDtypeStruct(x.shape, jnp.bf...  5.29 us
  transfers between devices with their start and end apart: 3, of which 2 were waited for; matrix products, arithmetic and copies ran while one was open for 5% of the time, Pallas kernels for 0%

profile of v2, /device:TPU:32, one launch (start us, length us, event | category | flops | bytes accessed | tf_op | source)
XLA Modules:
  0.0 185.6 jit_solution(145049896710292584)
XLA Ops:
  0.0 2.0 %broadcast_in_dim.30 = bf16[16,256,128]{2,1,0:T(8,128)(2,1)} broadcast(bf16[256,128]{1,0:T(8,128)(2,1)} %param.16), dimensions={1,2} | broadcast | bytes 1114112 | tf_op jit(solution)/shard_map/broadcast_in_dim | solution.py:111
  2.0 7.0 %all-to-all-start = ((bf16[16,256,128]{2,1,0:T(8,128)(2,1)}), bf16[16,256,128]{2,1,0:T(8,128)(2,1)S(1)}, u32[]{:S(2)}, u32[]{:S(2)}) async-start(bf16[16,256,128]{2,1,0:T(8,128)(2,1)} %broadcast_in_dim.30), calls=%async_computation | async-start | bytes 2097152 | tf_op jit(solution)/shard_map/all_to_all | solution.py:107
  9.1 0.0 copy-start.2
  9.1 0.9 copy-done.2
  10.0 0.0 copy-start.3
  10.0 0.9 copy-done.3
  10.9 0.0 copy-start.4
  10.9 0.9 copy-done.4
  11.8 0.0 copy-start.5
  11.8 0.9 copy-done.5
  12.7 0.0 copy-start.6
  12.7 0.9 copy-done.6
  13.6 0.0 copy-start.7
  13.6 0.9 copy-done.7
  14.5 0.1 convert_element_type.21
  14.6 0.0 copy-start.13
  14.6 0.0 copy-start.14
  14.6 71.9 %all-gather.1 = f16[2048,2304]{1,0:T(8,128)(2,1)} all-gather(f16[64,2304]{1,0:T(8,128)(2,1)S(1)} %convert_element_type.21), channel_id=1, replica_groups=mesh['ra_0'=4,'ra_1'=4,'cb_0'=16,'cb_1'=2] {'cb_0','cb_1'}, dimensions={0}, use_global_device_ids=true | all-gather | bytes 9732096 | tf_op jit(solution)/shard_map/all_gather | solution.py:143
  86.5 0.0 copy-done.13
  86.5 0.0 copy-done.14
  86.5 0.0 copy-start.8
  86.5 8.9 %slice_convert_fusion = (bf16[2048,1152]{1,0:T(8,128)(2,1)}, bf16[2048,1152]{1,0:T(8,128)(2,1)}) fusion(f16[2048,2304]{1,0:T(8,128)(2,1)} %all-gather.1), kind=kLoop, calls=%fused_computation | loop fusion | flops 4718592 | bytes 18874368 | tf_op jit(solution)/shard_map/convert_element_type | solution.py:148
  95.5 0.0 all-to-all-done.pieces
  95.5 0.0 copy-done.8
  95.5 0.9 shard_map.154.x
  96.4 0.0 copy-start.1
  96.4 2.3 %copy-done.1 = bf16[2048,1152]{1,0:T(8,128)(2,1)S(1)} copy-done((bf16[2048,1152]{1,0:T(8,128)(2,1)S(1)}, bf16[2048,1152]{1,0:T(8,128)(2,1)}, u32[]{:S(2)}) %copy-start.1) | copy-done | bytes 4718616
  98.7 0.0 copy-start.9
  98.7 3.2 %shard_map.156 = bf16[256,2048]{1,0:T(8,128)(2,1)} custom-call(bf16[256,2048]{1,0:T(8,128)(2,1)S(1)} %shard_map.154.x, bf16[2048,1152]{1,0:T(8,128)(2,1)S(1)} %copy-done.1, f32[1,384]{1,0:T(1,128)S(1)} %broadcast_in_dim.32.s_gate, f32[1,384]{1,0:T(1,128)S(1)} %broadcast_in_dim.33.s_up), custom_call_target="tpu_custom_call" | custom-call | tf_op jit(solution)/shard_map/pallas_call | solution.py:70
  101.9 7.1 %all-to-all-start.1 = ((bf16[16,16,2048]{2,1,0:T(8,128)(2,1)}), bf16[16,16,2048]{2,1,0:T(8,128)(2,1)S(1)}, u32[]{:S(2)}, u32[]{:S(2)}) async-start(bf16[16,16,2048]{2,1,0:T(8,128)(2,1)} %bitcast.3), calls=%async_computation.1 | async-start | bytes 2097152 | tf_op jit(solution)/shard_map/all_to_all | solution.py:107
  109.1 18.2 %all-to-all-done.1.pieces = bf16[16,16,2048]{2,1,0:T(8,128)(2,1)S(1)} async-done(((bf16[16,16,2048]{2,1,0:T(8,128)(2,1)}), bf16[16,16,2048]{2,1,0:T(8,128)(2,1)S(1)}, u32[]{:S(2)}, u32[]{:S(2)}) %all-to-all-start.1) | async-done | bytes 1048608 | tf_op jit(solution)/shard_map/all_to_all | solution.py:107
  127.3 0.0 copy-done.9
  127.3 0.0 copy-done.10
  127.3 1.3 shard_map.157
  128.6 3.7 %all-to-all-start.2 = ((bf16[16,16,2048]{2,1,0:T(8,128)(2,1)}), bf16[16,16,2048]{2,1,0:T(8,128)(2,1)S(1)}, u32[]{:S(2)}, u32[]{:S(2)}) async-start(bf16[16,16,2048]{2,1,0:T(8,128)(2,1)} %get-tuple-element.8), calls=%async_computation.2 | async-start | bytes 2097152 | tf_op jit(solution)/shard_map/all_to_all | solution.py:107
  132.2 0.0 copy-done.15
  132.2 0.0 copy-start.11
  132.2 0.0 copy-start.12
  132.3 0.0 copy-done.16
  132.3 17.3 %all-to-all-done.2 = bf16[16,16,2048]{2,1,0:T(8,128)(2,1)S(1)} async-done(((bf16[16,16,2048]{2,1,0:T(8,128)(2,1)}), bf16[16,16,2048]{2,1,0:T(8,128)(2,1)S(1)}, u32[]{:S(2)}, u32[]{:S(2)}) %all-to-all-start.2) | async-done | bytes 1048608 | tf_op jit(solution)/shard_map/all_to_all | solution.py:107
  149.7 2.3 %copy-done = bf16[2048,1152]{1,0:T(8,128)(2,1)S(1)} copy-done((bf16[2048,1152]{1,0:T(8,128)(2,1)S(1)}, bf16[2048,1152]{1,0:T(8,128)(2,1)}, u32[]{:S(2)}) %copy-start) | copy-done | bytes 4718616
  152.0 2.1 %shard_map.158 = bf16[256,2048]{1,0:T(8,128)(2,1)S(1)} custom-call(bf16[256,2048]{1,0:T(8,128)(2,1)S(1)} %bitcast.24, bf16[2048,1152]{1,0:T(8,128)(2,1)S(1)} %copy-done, f32[1,384]{1,0:T(1,128)S(1)} %broadcast_in_dim.36.s_gate, f32[1,384]{1,0:T(1,128)S(1)} %broadcast_in_dim.37.s_up), custom_call_target="tpu_custom_call" | custom-call | tf_op jit(solution)/shard_map/pallas_call | solution.py:70
  154.1 19.4 %all_to_all.25.pieces = bf16[16,16,2048]{2,1,0:T(8,128)(2,1)S(1)} all-to-all(bf16[16,16,2048]{2,1,0:T(8,128)(2,1)S(1)} %bitcast.25), channel_id=1, replica_groups=mesh['ra_0'=4,'ra_1'=4,'cb_0'=16,'cb_1'=2] {'ra_0','ra_1'}, dimensions={0} | all-to-all | bytes 2097152 | tf_op jit(solution)/shard_map/all_to_all | solution.py:107
  173.5 0.0 copy-done.11
  173.5 0.0 copy-done.12
  173.5 0.8 shard_map.159
  174.3 10.6 %all_to_all.26 = bf16[16,16,128]{2,1,0:T(8,128)(2,1)S(1)} all-to-all(bf16[16,16,128]{2,1,0:T(8,128)(2,1)S(1)} %bitcast_bitcast_fusion), channel_id=1, replica_groups=mesh['ra_0'=4,'ra_1'=4,'cb_0'=16,'cb_1'=2] {'ra_0','ra_1'}, dimensions={0} | all-to-all | bytes 131072 | tf_op jit(solution)/shard_map/all_to_all | solution.py:107
  185.0 0.6 copy.26
  (19 shorter events, 0.1 us)
Async XLA Ops:
  2.0 93.4 %all-to-all-start = ((bf16[16,256,128]{2,1,0:T(8,128)(2,1)}), bf16[16,256,128]{2,1,0:T(8,128)(2,1)S(1)}, u32[]{:S(2)}, u32[]{:S(2)}) async-start(bf16[16,256,128]{2,1,0:T(8,128)(2,1)} %broadcast_in_dim.30), calls=%async_computation | async-start | bytes 2097152 | tf_op jit(solution)/shard_map/all_to_all | solution.py:107
  9.1 0.9 copy-start.2
  10.0 0.9 copy-start.3
  10.9 0.9 copy-start.4
  11.8 0.9 copy-start.5
  12.7 0.9 copy-start.6
  13.6 0.9 copy-start.7
  14.6 71.9 %copy-start.13 = (f32[352]{0:T(512)S(1)}, f32[352]{0:T(512)}, u32[]{:S(2)}) copy-start(f32[352]{0:T(512)} %param.19) | copy-start | bytes 4228
  14.6 71.9 %copy-start.14 = (f32[352]{0:T(512)S(1)}, f32[352]{0:T(512)}, u32[]{:S(2)}) copy-start(f32[352]{0:T(512)} %param.21) | copy-start | bytes 4228
  86.5 8.9 %copy-start.8 = (f32[2048]{0:T(1024)S(1)}, f32[2048]{0:T(1024)}, u32[]{:S(2)}) copy-start(f32[2048]{0:T(1024)} %param.17) | copy-start | bytes 24580
  96.4 2.3 %copy-start.1 = (bf16[2048,1152]{1,0:T(8,128)(2,1)S(1)}, bf16[2048,1152]{1,0:T(8,128)(2,1)}, u32[]{:S(2)}) copy-start(bf16[2048,1152]{1,0:T(8,128)(2,1)} %get-tuple-element.12.weights) | copy-start | bytes 14155780
  98.7 28.5 %copy-start.9 = (f32[2048]{0:T(1024)S(1)}, f32[2048]{0:T(1024)}, u32[]{:S(2)}) copy-start(f32[2048]{0:T(1024)} %param.23) | copy-start | bytes 24580
  98.7 28.5 %copy-start.10 = (f32[2048]{0:T(1024)S(1)}, f32[2048]{0:T(1024)}, u32[]{:S(2)}) copy-start(f32[2048]{0:T(1024)} %param.24) | copy-start | bytes 24580
  98.7 33.5 %copy-start.15 = (f32[352]{0:T(512)S(1)}, f32[352]{0:T(512)}, u32[]{:S(2)}) copy-start(f32[352]{0:T(512)} %param.26) | copy-start | bytes 4228
  98.7 33.6 %copy-start.16 = (f32[352]{0:T(512)S(1)}, f32[352]{0:T(512)}, u32[]{:S(2)}) copy-start(f32[352]{0:T(512)} %param.28) | copy-start | bytes 4228
  101.9 25.4 %all-to-all-start.1 = ((bf16[16,16,2048]{2,1,0:T(8,128)(2,1)}), bf16[16,16,2048]{2,1,0:T(8,128)(2,1)S(1)}, u32[]{:S(2)}, u32[]{:S(2)}) async-start(bf16[16,16,2048]{2,1,0:T(8,128)(2,1)} %bitcast.3), calls=%async_computation.1 | async-start | bytes 2097152 | tf_op jit(solution)/shard_map/all_to_all | solution.py:107
  128.6 21.1 %all-to-all-start.2 = ((bf16[16,16,2048]{2,1,0:T(8,128)(2,1)}), bf16[16,16,2048]{2,1,0:T(8,128)(2,1)S(1)}, u32[]{:S(2)}, u32[]{:S(2)}) async-start(bf16[16,16,2048]{2,1,0:T(8,128)(2,1)} %get-tuple-element.8), calls=%async_computation.2 | async-start | bytes 2097152 | tf_op jit(solution)/shard_map/all_to_all | solution.py:107
  132.2 41.3 %copy-start.11 = (f32[2048]{0:T(1024)S(1)}, f32[2048]{0:T(1024)}, u32[]{:S(2)}) copy-start(f32[2048]{0:T(1024)} %param.30) | copy-start | bytes 24580
  132.2 41.3 %copy-start.12 = (f32[2048]{0:T(1024)S(1)}, f32[2048]{0:T(1024)}, u32[]{:S(2)}) copy-start(f32[2048]{0:T(1024)} %param.31) | copy-start | bytes 24580
  149.7 2.3 %copy-start = (bf16[2048,1152]{1,0:T(8,128)(2,1)S(1)}, bf16[2048,1152]{1,0:T(8,128)(2,1)}, u32[]{:S(2)}) copy-start(bf16[2048,1152]{1,0:T(8,128)(2,1)} %get-tuple-element.11.weights) | copy-start | bytes 14155780

commit v3 on v2

v3 whole, which is shorter than its diff:
```python
import functools

import jax
import jax.numpy as jnp
from jax import lax
from jax.experimental import pallas as pl
from jax.experimental.pallas import tpu as pltpu
from jax.sharding import Mesh
from jax.sharding import PartitionSpec as P


D = 2048
HALF = D // 2
RA = ("ra_0", "ra_1")
CB = ("cb_0", "cb_1")
LANES = 384
TILE = 128
EPS = 1e-06
LIFT = 2.0**18
ROOM = pltpu.CompilerParams(vmem_limit_bytes=20 * 1024 * 1024)
MOST = pltpu.CompilerParams(vmem_limit_bytes=50 * 1024 * 1024)
VMEM = pl.BlockSpec(memory_space=pltpu.VMEM)
HBM = pl.BlockSpec(memory_space=pltpu.HBM)


def pack_body(*refs):
    pieces, (out, held, sems) = refs[:6], refs[6:]
    loads = [pltpu.make_async_copy(p, held.at[j], sems.at[j]) for j, p in enumerate(pieces)]
    for load in loads:
        load.start()
    width = held.shape[2]
    out[...] = jnp.zeros_like(out)
    for j, load in enumerate(loads):
        load.wait()
        out[:, j * LANES : j * LANES + width] = held[j].astype(jnp.bfloat16) * LIFT


def pack(*pieces):
    rows, width = pieces[0].shape
    return pl.pallas_call(
        pack_body,
        in_specs=[HBM] * 6,
        out_shape=jax.ShapeDtypeStruct((rows, 6 * LANES), jnp.bfloat16),
        scratch_shapes=[
            pltpu.VMEM((6, rows, width), jnp.float32),
            pltpu.SemaphoreType.DMA((6,)),
        ],
    )(*pieces)


def halves(left, right):
    low = lax.broadcasted_iota(jnp.int32, left.shape, 1) < TILE // 2
    turn = functools.partial(pltpu.roll, shift=TILE // 2, axis=1)
    return jnp.where(low, left, turn(right)), jnp.where(low, turn(left), right)


def to_split(tiles):
    pairs = [halves(*tiles[j : j + 2]) for j in range(0, len(tiles), 2)]
    return [a for a, _ in pairs] + [b for _, b in pairs]


def from_split(tiles):
    count = len(tiles) // 2
    pairs = [halves(tiles[j], tiles[j + count]) for j in range(count)]
    return [tile for pair in pairs for tile in pair]


def tiles_of(value):
    return [value[:, j : j + TILE] for j in range(0, value.shape[1], TILE)]


def split_row(vector):
    rows = jnp.broadcast_to(vector[...], (8, D))
    return jnp.concatenate(to_split(tiles_of(rows)), axis=1)[:1]


def spread_body(pieces, gain, out, own):
    count, rows, _ = pieces.shape
    total = jnp.zeros((rows, 1), jnp.float32)
    for j in range(count):
        piece = pieces[j].astype(jnp.float32)
        total += jnp.sum(piece * piece, axis=1, keepdims=True)
    scale = lax.rsqrt(total / D + EPS)
    few = own.shape[0]
    start = pl.multiple_of(lax.axis_index(RA) * few, few)
    for j in range(0, count, 2):
        normed, kept = [], []
        for i in (j, j + 1):
            value = pieces[i].astype(jnp.float32)
            normed.append(value * scale * gain[:, i * TILE : (i + 1) * TILE])
            kept.append(pieces[i, pl.ds(start, few), :].astype(jnp.float32))
        for side in (0, 1):
            at = slice(side * HALF + j // 2 * TILE, side * HALF + (j // 2 + 1) * TILE)
            out[:, at] = halves(*normed)[side].astype(jnp.bfloat16)
            own[:, at] = halves(*kept)[side]


def spread(pieces, gain):
    count, rows, _ = pieces.shape
    return pl.pallas_call(
        spread_body,
        out_shape=(
            jax.ShapeDtypeStruct((rows, D), jnp.bfloat16),
            jax.ShapeDtypeStruct((rows // count, D), jnp.float32),
        ),
        compiler_params=ROOM,
    )(pieces, gain[None])


def block_body(x, near, far, s_gate, s_up, out, held, scales, sems):
    loads = [
        [
            pltpu.make_async_copy(
                weights.at[:, pl.ds(j * LANES, LANES)],
                held.at[side, :, pl.ds(j * LANES, LANES)],
                sems.at[side, j],
            )
            for side, weights in enumerate((near, far))
        ]
        for j in range(3)
    ]
    for pair in loads:
        for load in pair:
            load.start()
    scales[...] = jnp.zeros_like(scales)
    scales[0:1, : s_gate.shape[1]] = s_gate[...] / LIFT
    scales[1:2, : s_up.shape[1]] = s_up[...] / LIFT
    core = lax.axis_index("cb_1")
    columns = [
        pl.ds(pl.multiple_of(core * HALF, HALF), HALF),
        pl.ds(pl.multiple_of((1 - core) * HALF, HALF), HALF),
    ]

    def product(j):
        parts = []
        for side in (0, 1):
            loads[j][side].wait()
            part = held[side, :, j * LANES : (j + 1) * LANES]
            parts.append(jnp.dot(x[:, columns[side]], part, preferred_element_type=jnp.float32))
        return (parts[0] + parts[1]) * scales[j : j + 1]

    gate = product(0)
    upper = product(1)
    hidden = (gate / (1.0 + jnp.exp(-gate)) * upper).astype(jnp.bfloat16)
    for side in (0, 1):
        loads[2][side].wait()
        out[:, columns[side]] = lax.dot_general(
            hidden,
            held[side, :, 2 * LANES :],
            (((1,), (1,)), ((), ())),
            preferred_element_type=jnp.float32,
        ).astype(jnp.bfloat16)


def block(x, near, far, s_gate, s_up):
    return pl.pallas_call(
        block_body,
        in_specs=[VMEM, HBM, HBM, VMEM, VMEM],
        out_shape=jax.ShapeDtypeStruct(x.shape, jnp.bfloat16),
        scratch_shapes=[
            pltpu.VMEM((2, *near.shape), jnp.bfloat16),
            pltpu.VMEM((8, LANES), jnp.float32),
            pltpu.SemaphoreType.DMA((2, 3)),
        ],
        compiler_params=MOST,
    )(x, near, far, s_gate[None], s_up[None])


def join_body(last, pieces, before, scale, gain, *outs):
    count = pieces.shape[0]
    added = pieces[0].astype(jnp.float32)
    for j in range(1, count):
        added += pieces[j].astype(jnp.float32)
    values = 0.1 * before[...] + (0.5 / LIFT) * added * split_row(scale)
    meansq = jnp.sum(values * values, axis=1, keepdims=True) / D
    normed = values * lax.rsqrt(meansq + EPS) * split_row(gain)
    if last:
        (out,) = outs
        for j, tile in enumerate(from_split(tiles_of(normed))):
            out[j] = tile.astype(jnp.bfloat16)
    else:
        out, total = outs
        total[...] = values
        for j in range(count):
            out[j] = normed.astype(jnp.bfloat16)


def join(pieces, before, scale, gain, last):
    count, rows, _ = pieces.shape
    shapes = [jax.ShapeDtypeStruct((count, rows, TILE if last else D), jnp.bfloat16)]
    if not last:
        shapes.append(jax.ShapeDtypeStruct((rows, D), jnp.float32))
    return pl.pallas_call(
        functools.partial(join_body, last), out_shape=shapes, compiler_params=ROOM
    )(pieces, before, scale[None], gain[None])


def exchange(pieces):
    return lax.all_to_all(pieces, RA, split_axis=0, concat_axis=0, tiled=True)


def copy_for_each(x):
    return exchange(jnp.broadcast_to(x, (lax.axis_size(RA), *x.shape)))


def by_rows(partial_value):
    return exchange(partial_value.reshape(lax.axis_size(RA), -1, D))


def both_cores(weights):
    near = weights.astype(jnp.bfloat16)
    return near, lax.ppermute(near, "cb_1", ((0, 1), (1, 0)))


def shards(
    tokens,
    gain_first,
    gate_first,
    gate_first_scale,
    up_first,
    up_first_scale,
    down_first,
    down_first_scale,
    gain_second,
    gate_second,
    gate_second_scale,
    up_second,
    up_second_scale,
    down_second,
    down_second_scale,
    gain_last,
):
    packed = pack(gate_first, up_first, down_first.T, gate_second, up_second, down_second.T)
    packed, tokens = lax.optimization_barrier((packed, tokens))
    pieces = copy_for_each(tokens)
    packed = packed.astype(jnp.float16)
    weights = lax.all_gather(packed, "cb_0", axis=0, tiled=True)
    near, far = both_cores(weights[:, : 3 * LANES])
    normed, own = spread(pieces, gain_first)
    partial_first = block(normed, near, far, gate_first_scale, up_first_scale)
    weights, partial_first = lax.optimization_barrier((weights, partial_first))
    near, far = both_cores(weights[:, 3 * LANES :])
    arrived = by_rows(partial_first)
    copies, first = join(arrived, own, down_first_scale, gain_second, False)
    normed = exchange(copies).reshape(-1, D)
    partial_second = block(normed, near, far, gate_second_scale, up_second_scale)
    (columns,) = join(by_rows(partial_second), first, down_second_scale, gain_last, True)
    return exchange(columns).reshape(tokens.shape)


def solution(mesh):
    torus = Mesh(mesh.devices.reshape(4, 4, 16, 2), ("ra_0", "ra_1", "cb_0", "cb_1"))
    weight, across = P(CB, RA), P(RA, CB)
    return jax.shard_map(
        shards,
        mesh=torus,
        in_specs=(
            P(CB, RA),
            P(),
            weight,
            P(RA),
            weight,
            P(RA),
            across,
            P(),
            P(),
            weight,
            P(RA),
            weight,
            P(RA),
            across,
            P(),
            P(),
        ),
        out_specs=P(CB, RA),
        check_vma=False,
    )
```

time: 186 us -> 191 us (1.027)
  blocking collectives: 102 us -> 122 us
  local copies, waits for them, and re-layouts: 12.8 us -> 3.64 us
  other arithmetic: 9.01 us -> 1.75 us
  Pallas kernels: 8.34 us -> 12.8 us
  starting transfers between devices: 17.8 us -> 14.7 us
    all_to_all x2 -> x3, blocking collectives: 30 us -> 50.6 us  [exchange(): return lax.all_to_all(pieces, RA, split_axis=0, concat_axis=0, tiled=True)]
    unnamed x35 -> x29, local copies, waits for them, and re-layouts: 10.7 us -> 2.43 us
    convert_element_type x3, other arithmetic: 9 us -> 1.75 us  [the longest x1 1.01 us: shards(): packed = packed.astype(jnp.float16)]
    all_to_all x3 -> x2, starting transfers between devices: 17.8 us -> 10.7 us  [exchange(): return lax.all_to_all(pieces, RA, split_axis=0, concat_axis=0, tiled=True)]
    pallas_call x6, Pallas kernels: 8.34 us -> 12.8 us  [the longest x2 8.04 us: block(): pl.pallas_call(block_body, in_specs=[VMEM, HBM, HBM, VMEM, VMEM], out_sha...]
    ppermute x0 -> x2, starting transfers between devices: none -> 3.97 us  [both_cores(): return (near, lax.ppermute(near, 'cb_1', ((0, 1), (1, 0))))]
    all_to_all x3 -> x2, waiting for transfers between devices: 35.5 us -> 35.5 us  [exchange(): return lax.all_to_all(pieces, RA, split_axis=0, concat_axis=0, tiled=True)]
  transfers between devices with their start and end apart: 3 -> 4, of which waited for: 2 -> 2; matrix products, arithmetic and copies ran while one was open for 5% -> 1% of each run, Pallas kernels for 0% -> 1%
where the time goes in v3:
time: 191 us; the launch traced here: 190 us
  blocking collectives  122 us (64%)
  waiting for transfers between devices  35.5 us (19%)
  starting transfers between devices  14.7 us (8%)
  Pallas kernels  12.8 us (7%)
  local copies, waits for them, and re-layouts  3.64 us (2%)
    all_gather x1, blocking collectives, shards(): weights = lax.all_gather(packed, 'cb_0', axis=0, tiled=True)  71 us
    all_to_all x3, blocking collectives, exchange(): return lax.all_to_all(pieces, RA, split_axis=0, concat_axis=0, tiled=True)  50.6 us
    all_to_all x2, waiting for transfers between devices, exchange(): return lax.all_to_all(pieces, RA, split_axis=0, concat_axis=0, tiled=True)  35.5 us
    all_to_all x2, starting transfers between devices, exchange(): return lax.all_to_all(pieces, RA, split_axis=0, concat_axis=0, tiled=True)  10.7 us
    pallas_call x2, Pallas kernels, block(): pl.pallas_call(block_body, in_specs=[VMEM, HBM, HBM, VMEM, VMEM], out_sha...  8.04 us
    ppermute x2, starting transfers between devices, both_cores(): return (near, lax.ppermute(near, 'cb_1', ((0, 1), (1, 0))))  3.97 us
  transfers between devices with their start and end apart: 4, of which 2 were waited for; matrix products, arithmetic and copies ran while one was open for 1% of the time, Pallas kernels for 1%

profile of v3, /device:TPU:32, one launch (start us, length us, event | category | flops | bytes accessed | tf_op | source)
XLA Modules:
  0.0 190.1 jit_solution(14502349359988899407)
XLA Ops:
  0.0 1.9 %shard_map.154 = bf16[64,2304]{1,0:T(8,128)(2,1)} custom-call(f32[64,352]{1,0:T(8,128)} %refs_0_.1, f32[64,352]{1,0:T(8,128)} %refs_1_.1, f32[64,352]{1,0:T(8,128)} %bitcast.20, f32[64,352]{1,0:T(8,128)} %refs_3_.1, f32[64,352]{1,0:T(8,128)} %refs_4_.1, f32[64,352]{1,0:T(8,128)} %bitcast.21), custom_call_target="tpu_custom_call" | custom-call | tf_op jit(solution)/shard_map/pallas_call | solution.py:40
  1.9 1.0 convert_element_type.9
  2.9 71.0 %all-gather.1 = f16[1024,2304]{1,0:T(8,128)(2,1)S(1)} all-gather(f16[64,2304]{1,0:T(8,128)(2,1)S(1)} %convert_element_type.9), channel_id=1, replica_groups=mesh['ra_0'=4,'ra_1'=4,'cb_0'=16,'cb_1'=2] {'cb_0'}, dimensions={0}, use_global_device_ids=true | all-gather | bytes 5013504 | tf_op jit(solution)/shard_map/all_gather | solution.py:237
  73.9 0.0 copy-start.9
  73.9 0.4 slice_convert_fusion.near
  74.3 1.7 copy-done.5
  76.0 0.0 copy-start.8
  76.0 0.0 copy-start.10
  76.0 0.0 copy-start.11
  76.0 0.0 copy-start
  76.0 2.1 %collective-permute-start = (bf16[1024,1152]{1,0:T(8,128)(2,1)S(1)}, bf16[1024,1152]{1,0:T(8,128)(2,1)}, u32[]{:S(2)}, u32[]{:S(2)}) collective-permute-start(bf16[1024,1152]{1,0:T(8,128)(2,1)S(1)} %slice_convert_fusion.near), channel_id=1, source_target_pairs={{0,1},{1,0},{2,3},{3,2},{4,5},{5,4},{6,7},{7,6},{8,9},{9,8},{10,11... | collective-permute-start | bytes 7077896 | tf_op jit(solution)/shard_map/ppermute | solution.py:212
  78.1 0.0 copy-done.9
  78.1 1.2 broadcast_in_dim.30
  79.3 7.0 %all-to-all-start = ((bf16[16,256,128]{2,1,0:T(8,128)(2,1)}), bf16[16,256,128]{2,1,0:T(8,128)(2,1)S(1)}, u32[]{:S(2)}, u32[]{:S(2)}) async-start(bf16[16,256,128]{2,1,0:T(8,128)(2,1)} %broadcast_in_dim.30), calls=%async_computation | async-start | bytes 2097152 | tf_op jit(solution)/shard_map/all_to_all | solution.py:199
  86.4 0.0 copy-done.10
  86.4 0.0 copy-done.11
  86.4 18.5 %all-to-all-done.pieces = bf16[16,256,128]{2,1,0:T(8,128)(2,1)S(1)} async-done(((bf16[16,256,128]{2,1,0:T(8,128)(2,1)}), bf16[16,256,128]{2,1,0:T(8,128)(2,1)S(1)}, u32[]{:S(2)}, u32[]{:S(2)}) %all-to-all-start) | async-done | bytes 1048608 | tf_op jit(solution)/shard_map/all_to_all | solution.py:199
  104.9 0.0 copy-done
  104.9 1.1 shard_map.155
  106.1 0.0 collective-permute-done.far
  106.1 0.0 copy-done.8
  106.1 0.0 copy-start.6
  106.1 4.1 %shard_map.156 = bf16[256,2048]{1,0:T(8,128)(2,1)S(1)} custom-call(bf16[256,2048]{1,0:T(8,128)(2,1)S(1)} %get-tuple-element.15.x, bf16[1024,1152]{1,0:T(8,128)(2,1)} %copy-done.8, bf16[1024,1152]{1,0:T(8,128)(2,1)} %collective-permute-done.far, f32[1,352]{1,0:T(1,128)S(1)} %broadcast_in_dim.32.s_gate, f32[1,352]{1,0:T(1,128)S(1)} %broadcast_in_dim.33.s_up), custom_call_target="tpu_custom_call" | custom-call | tf_op jit(solution)/shard_map/pallas_call | solution.py:156
  110.2 0.0 copy-done.6
  110.2 0.0 copy-start.1
  110.2 0.0 copy-start.2
  110.2 0.3 slice_convert_fusion.1.near
  110.6 0.0 copy-start.7
  110.6 1.9 %collective-permute-start.1 = (bf16[1024,1152]{1,0:T(8,128)(2,1)S(1)}, bf16[1024,1152]{1,0:T(8,128)(2,1)}, u32[]{:S(2)}, u32[]{:S(2)}) collective-permute-start(bf16[1024,1152]{1,0:T(8,128)(2,1)S(1)} %slice_convert_fusion.1.near), channel_id=1, source_target_pairs={{0,1},{1,0},{2,3},{3,2},{4,5},{5,4},{6,7},{7,6},{8,9},{9,8},{10,11... | collective-permute-start | bytes 7077896 | tf_op jit(solution)/shard_map/ppermute | solution.py:212
  112.5 0.0 copy-start.12
  112.5 0.0 copy-start.13
  112.6 20.8 %all_to_all.25.pieces = bf16[16,16,2048]{2,1,0:T(8,128)(2,1)S(1)} all-to-all(bf16[16,16,2048]{2,1,0:T(8,128)(2,1)S(1)} %bitcast.12), channel_id=1, replica_groups=mesh['ra_0'=4,'ra_1'=4,'cb_0'=16,'cb_1'=2] {'ra_0','ra_1'}, dimensions={0} | all-to-all | bytes 2097152 | tf_op jit(solution)/shard_map/all_to_all | solution.py:199
  133.3 0.0 copy-done.1
  133.3 0.0 copy-done.2
  133.3 1.4 shard_map.157
  134.7 0.0 copy-done.7
  134.7 3.7 %all-to-all-start.2 = ((bf16[16,16,2048]{2,1,0:T(8,128)(2,1)}), bf16[16,16,2048]{2,1,0:T(8,128)(2,1)S(1)}, u32[]{:S(2)}, u32[]{:S(2)}) async-start(bf16[16,16,2048]{2,1,0:T(8,128)(2,1)} %get-tuple-element.18), calls=%async_computation.2 | async-start | bytes 2097152 | tf_op jit(solution)/shard_map/all_to_all | solution.py:199
  138.3 0.0 copy-done.12
  138.4 0.0 copy-done.13
  138.4 17.0 %all-to-all-done.2 = bf16[16,16,2048]{2,1,0:T(8,128)(2,1)S(1)} async-done(((bf16[16,16,2048]{2,1,0:T(8,128)(2,1)}), bf16[16,16,2048]{2,1,0:T(8,128)(2,1)S(1)}, u32[]{:S(2)}, u32[]{:S(2)}) %all-to-all-start.2) | async-done | bytes 1048608 | tf_op jit(solution)/shard_map/all_to_all | solution.py:199
  155.4 0.0 collective-permute-done.1.far
  155.4 4.0 %shard_map.158 = bf16[256,2048]{1,0:T(8,128)(2,1)S(1)} custom-call(bf16[256,2048]{1,0:T(8,128)(2,1)S(1)} %bitcast.11, bf16[1024,1152]{1,0:T(8,128)(2,1)} %copy-done.7, bf16[1024,1152]{1,0:T(8,128)(2,1)} %collective-permute-done.1.far, f32[1,352]{1,0:T(1,128)S(1)} %broadcast_in_dim.36.s_gate, f32[1,352]{1,0:T(1,128)S(1)} %broadcast_in_dim.37.s_up), custom_call_target="tpu_custom_call" | custom-call | tf_op jit(solution)/shard_map/pallas_call | solution.py:156
  159.3 19.2 %all_to_all.26.pieces = bf16[16,16,2048]{2,1,0:T(8,128)(2,1)S(1)} all-to-all(bf16[16,16,2048]{2,1,0:T(8,128)(2,1)S(1)} %bitcast.13), channel_id=1, replica_groups=mesh['ra_0'=4,'ra_1'=4,'cb_0'=16,'cb_1'=2] {'ra_0','ra_1'}, dimensions={0} | all-to-all | bytes 2097152 | tf_op jit(solution)/shard_map/all_to_all | solution.py:199
  178.5 0.0 copy-done.3
  178.5 0.0 copy-done.4
  178.5 0.3 shard_map.159
  178.9 10.6 %all_to_all.27 = bf16[16,16,128]{2,1,0:T(8,128)(2,1)S(1)} all-to-all(bf16[16,16,128]{2,1,0:T(8,128)(2,1)S(1)} %shard_map.159), channel_id=1, replica_groups=mesh['ra_0'=4,'ra_1'=4,'cb_0'=16,'cb_1'=2] {'ra_0','ra_1'}, dimensions={0} | all-to-all | bytes 131072 | tf_op jit(solution)/shard_map/all_to_all | solution.py:199
  189.5 0.6 copy.18
  (7 shorter events, 0.0 us)
Async XLA Ops:
  73.9 2.1 %copy-start.5 = (f16[1024,2304]{1,0:T(8,128)(2,1)}, f16[1024,2304]{1,0:T(8,128)(2,1)S(1)}, u32[]{:S(2)}) copy-start(f16[1024,2304]{1,0:T(8,128)(2,1)S(1)} %all-gather.1) | copy-start | bytes 14155780
  73.9 4.2 %copy-start.9 = (bf16[256,128]{1,0:T(8,128)(2,1)S(1)}, bf16[256,128]{1,0:T(8,128)(2,1)}, u32[]{:S(2)}) copy-start(bf16[256,128]{1,0:T(8,128)(2,1)} %param.16) | copy-start | bytes 196612
  76.0 30.1 %copy-start.8 = (bf16[1024,1152]{1,0:T(8,128)(2,1)}, bf16[1024,1152]{1,0:T(8,128)(2,1)S(1)}, u32[]{:S(2)}) copy-start(bf16[1024,1152]{1,0:T(8,128)(2,1)S(1)} %slice_convert_fusion.near) | copy-start | bytes 7077892
  76.0 10.3 %copy-start.10 = (f32[352]{0:T(512)S(1)}, f32[352]{0:T(512)}, u32[]{:S(2)}) copy-start(f32[352]{0:T(512)} %param.19) | copy-start | bytes 4228
  76.0 10.3 %copy-start.11 = (f32[352]{0:T(512)S(1)}, f32[352]{0:T(512)}, u32[]{:S(2)}) copy-start(f32[352]{0:T(512)} %param.21) | copy-start | bytes 4228
  76.0 28.9 %copy-start = (f32[2048]{0:T(1024)S(1)}, f32[2048]{0:T(1024)}, u32[]{:S(2)}) copy-start(f32[2048]{0:T(1024)} %param.17) | copy-start | bytes 24580
  76.0 30.0 %collective-permute-start = (bf16[1024,1152]{1,0:T(8,128)(2,1)S(1)}, bf16[1024,1152]{1,0:T(8,128)(2,1)}, u32[]{:S(2)}, u32[]{:S(2)}) collective-permute-start(bf16[1024,1152]{1,0:T(8,128)(2,1)S(1)} %slice_convert_fusion.near), channel_id=1, source_target_pairs={{0,1},{1,0},{2,3},{3,2},{4,5},{5,4},{6,7},{7,6},{8,9},{9,8},{10,11... | collective-permute-start | bytes 7077896 | tf_op jit(solution)/shard_map/ppermute | solution.py:212
  79.3 25.6 %all-to-all-start = ((bf16[16,256,128]{2,1,0:T(8,128)(2,1)}), bf16[16,256,128]{2,1,0:T(8,128)(2,1)S(1)}, u32[]{:S(2)}, u32[]{:S(2)}) async-start(bf16[16,256,128]{2,1,0:T(8,128)(2,1)} %broadcast_in_dim.30), calls=%async_computation | async-start | bytes 2097152 | tf_op jit(solution)/shard_map/all_to_all | solution.py:199
  106.1 4.1 %copy-start.6 = (f16[1024,2304]{1,0:T(8,128)(2,1)S(1)}, f16[1024,2304]{1,0:T(8,128)(2,1)}, u32[]{:S(2)}) copy-start(f16[1024,2304]{1,0:T(8,128)(2,1)} %copy-done.5) | copy-start | bytes 14155780
  110.2 23.1 %copy-start.1 = (f32[2048]{0:T(1024)S(1)}, f32[2048]{0:T(1024)}, u32[]{:S(2)}) copy-start(f32[2048]{0:T(1024)} %param.23) | copy-start | bytes 24580
  110.2 23.1 %copy-start.2 = (f32[2048]{0:T(1024)S(1)}, f32[2048]{0:T(1024)}, u32[]{:S(2)}) copy-start(f32[2048]{0:T(1024)} %param.24) | copy-start | bytes 24580
  110.6 24.1 %copy-start.7 = (bf16[1024,1152]{1,0:T(8,128)(2,1)}, bf16[1024,1152]{1,0:T(8,128)(2,1)S(1)}, u32[]{:S(2)}) copy-start(bf16[1024,1152]{1,0:T(8,128)(2,1)S(1)} %slice_convert_fusion.1.near) | copy-start | bytes 7077892
  110.6 44.8 %collective-permute-start.1 = (bf16[1024,1152]{1,0:T(8,128)(2,1)S(1)}, bf16[1024,1152]{1,0:T(8,128)(2,1)}, u32[]{:S(2)}, u32[]{:S(2)}) collective-permute-start(bf16[1024,1152]{1,0:T(8,128)(2,1)S(1)} %slice_convert_fusion.1.near), channel_id=1, source_target_pairs={{0,1},{1,0},{2,3},{3,2},{4,5},{5,4},{6,7},{7,6},{8,9},{9,8},{10,11... | collective-permute-start | bytes 7077896 | tf_op jit(solution)/shard_map/ppermute | solution.py:212
  112.5 25.8 %copy-start.12 = (f32[352]{0:T(512)S(1)}, f32[352]{0:T(512)}, u32[]{:S(2)}) copy-start(f32[352]{0:T(512)} %param.26) | copy-start | bytes 4228
  112.5 25.8 %copy-start.13 = (f32[352]{0:T(512)S(1)}, f32[352]{0:T(512)}, u32[]{:S(2)}) copy-start(f32[352]{0:T(512)} %param.28) | copy-start | bytes 4228
  134.7 20.7 %all-to-all-start.2 = ((bf16[16,16,2048]{2,1,0:T(8,128)(2,1)}), bf16[16,16,2048]{2,1,0:T(8,128)(2,1)S(1)}, u32[]{:S(2)}, u32[]{:S(2)}) async-start(bf16[16,16,2048]{2,1,0:T(8,128)(2,1)} %get-tuple-element.18), calls=%async_computation.2 | async-start | bytes 2097152 | tf_op jit(solution)/shard_map/all_to_all | solution.py:199
  155.4 23.2 %copy-start.3 = (f32[2048]{0:T(1024)S(1)}, f32[2048]{0:T(1024)}, u32[]{:S(2)}) copy-start(f32[2048]{0:T(1024)} %param.30) | copy-start | bytes 24580
  155.4 23.2 %copy-start.4 = (f32[2048]{0:T(1024)S(1)}, f32[2048]{0:T(1024)}, u32[]{:S(2)}) copy-start(f32[2048]{0:T(1024)} %param.31) | copy-start | bytes 24580
